TPU v7x, 32 devices: a whole 2x2x4 slice. The times are simulated.
32 devices in a mesh: gr: 2 (over x), sp: 8 (over z, y), tp: 2 (over core).
Axes of the slice: x: 2, y: 2, z: 4, core: 2. Of those that a mesh axis runs over, the one named last changes fastest.
Arguments:
- tokens: bfloat16 [16, 512, 4096], P('gr', 'sp'), may hold values from -6 to 6
- key_weight: bfloat16 [4096, 2048], P(('gr', 'sp'), 'tp'), may hold values from -0.09375 to 0.09375
- value_weight: bfloat16 [4096, 2048], P(('gr', 'sp'), 'tp'), may hold values from -0.09375 to 0.09375
- gate_weight: bfloat16 [4096, 16], P(('gr', 'sp'), 'tp'), may hold values from -0.09375 to 0.09375
- forget_bias: float32 [16], P('tp'), may hold values from 7 to 9
- new_query: bfloat16 [16, 16, 128], P('gr', 'tp'), may hold values from -6 to 6
Outputs:
- key_cache: bfloat16 [16, 16, 512, 128], P(('gr', 'sp'), 'tp')
- value_cache: bfloat16 [16, 16, 512, 128], P(('gr', 'sp'), 'tp')
- gate_cache: float32 [16, 16, 512], P(('gr', 'sp'), 'tp')
- first_read: bfloat16 [16, 16, 128], P(('gr', 'sp'), 'tp')
All inputs are finite; a program needn't handle non-finite values.
Results may differ from a plain program's by a relative error of at most 0.0075.
Values may be sent and summed in bfloat16 or wider, within the bound.
A program may use at most 64 MiB of HBM per device.

v0:
```python
import jax
import jax.numpy as jnp
from jax import lax
from jax.sharding import PartitionSpec as P

eps = 1e-06


def taken_in(piece, axis, dim, turn, start):

    def gathered(part):
        return lax.all_gather(part, axis, axis=dim, tiled=True)

    return turn(start, jax.tree.map(gathered, piece), jnp.int32(0))


def carried_in(array, axis, combine, identity, reverse):
    length, mine = (lax.axis_size(axis), lax.axis_index(axis))
    everything = jax.tree.map(lambda part: lax.all_gather(part, axis), array)
    start = jax.tree.map(
        lambda part, zero: jnp.broadcast_to(jnp.asarray(zero, part.dtype), part.shape),
        array,
        identity,
    )

    def turn(k, before):
        at = length - 1 - k if reverse else k
        reached = at > mine if reverse else at < mine
        new = combine(before, jax.tree.map(lambda part: part[at], everything))
        return jax.tree.map(lambda a, b: jnp.where(reached, a, b), new, before)

    return lax.fori_loop(0, length, turn, start)


def add_pair(earlier, later):
    return earlier + later


def partial_read(queries, keys, values, cumulative, scaling):
    scores = (
        jnp.einsum("shd,shpd->shp", queries, keys, preferred_element_type=jnp.float32) * scaling
        - cumulative
    )
    highest = jnp.max(scores, axis=2)
    weights = jnp.exp(scores - highest[..., None])
    weight_sum = jnp.sum(weights, axis=2)
    value_sum = jnp.einsum("shp,shpd->shd", weights, values.astype(jnp.float32))
    return (highest, weight_sum, value_sum)


def on_device(tokens, key_weight, value_weight, gate_weight, forget_bias, new_query):
    sequences, positions, features = tokens.shape
    heads_here = forget_bias.shape[0]
    head_dim = new_query.shape[2]
    scaling = head_dim ** (-0.5)
    row_count = sequences * positions
    flat = tokens.reshape(row_count, features)
    empty_kv = jnp.zeros((row_count, key_weight.shape[1]), jnp.float32)
    empty_gate = jnp.zeros((row_count, heads_here), jnp.float32)
    initial = (empty_kv, empty_kv, empty_gate)

    def add_rows(sums, pieces, start):
        columns = lax.dynamic_slice_in_dim(flat, start, pieces[0].shape[0], 1)
        return tuple(
            (
                running + jnp.dot(columns, piece, preferred_element_type=jnp.float32)
                for running, piece in zip(sums, pieces)
            )
        )

    projected = taken_in(
        (key_weight, value_weight, gate_weight), ("gr", "sp"), 0, add_rows, initial
    )
    key_sum, value_sum, gate_logit = projected
    keys = (
        key_sum.astype(jnp.bfloat16)
        .reshape(sequences, positions, heads_here, head_dim)
        .transpose(0, 2, 1, 3)
    )
    values = (
        value_sum.astype(jnp.bfloat16)
        .reshape(sequences, positions, heads_here, head_dim)
        .transpose(0, 2, 1, 3)
    )
    log_gate = jax.nn.log_sigmoid(gate_logit + forget_bias).reshape(
        sequences, positions, heads_here
    )
    running_gate = jnp.cumsum(log_gate.transpose(0, 2, 1), axis=2)
    earlier_sum = carried_in(
        running_gate[:, :, -1],
        "sp",
        add_pair,
        jnp.zeros((sequences, heads_here), jnp.float32),
        False,
    )
    cumulative = running_gate + earlier_sum[:, :, None]
    key_cache, value_cache = (
        lax.all_to_all(keys, "sp", split_axis=0, concat_axis=2, tiled=True),
        lax.all_to_all(values, "sp", split_axis=0, concat_axis=2, tiled=True),
    )
    gate_cache = lax.all_to_all(cumulative, "sp", split_axis=0, concat_axis=2, tiled=True)
    member = lax.axis_index("sp")
    own_query = lax.dynamic_slice_in_dim(new_query, member, 1, 0)
    highest, weight_sum, value_total = partial_read(
        own_query, key_cache, value_cache, gate_cache, scaling
    )
    attended = value_total / weight_sum[..., None]
    normed = attended * lax.rsqrt(jnp.mean(attended * attended, axis=-1, keepdims=True) + eps)
    return (key_cache, value_cache, gate_cache, normed.astype(jnp.bfloat16))


def solution(mesh):
    in_specs = (
        P("gr", "sp", None),
        P(("gr", "sp"), "tp"),
        P(("gr", "sp"), "tp"),
        P(("gr", "sp"), "tp"),
        P("tp"),
        P("gr", "tp", None),
    )
    out_specs = (
        P(("gr", "sp"), "tp", None, None),
        P(("gr", "sp"), "tp", None, None),
        P(("gr", "sp"), "tp", None),
        P(("gr", "sp"), "tp", None),
    )
    return jax.shard_map(
        on_device, mesh=mesh, in_specs=in_specs, out_specs=out_specs, check_vma=False
    )
```

profile of v0, /device:TPU:0, one launch (start us, length us, event | category | flops | bytes accessed | tf_op | source)
XLA Modules:
  0.0 302.6 jit_solution(3733088857924785863)
XLA Ops:
  7.2 0.7 all-gather.4.cloned.1.call-update
  8.0 0.7 all-gather.6.cloned.1.call-update
  8.7 44.0 %all_gather.14 = bf16[4096,8]{0,1:T(8,128)(2,1)S(1)} all-gather(bf16[256,8]{0,1:T(8,128)(2,1)} %param.11), channel_id=1, replica_groups=mesh['gr'=2,'sp'=8,'tp'=2] {'gr','sp'}, dimensions={0}, use_global_device_ids=true | all-gather | bytes 69632 | tf_op jit(solution)/shard_map/all_gather | solution.py:12
  52.7 3.4 %fusion.7 = f32[512,8]{0,1:T(8,128)S(1)} fusion(bf16[512,4096]{1,0:T(8,128)(2,1)} %bitcast.73, bf16[4096,8]{0,1:T(8,128)(2,1)S(1)} %all_gather.14, f32[8]{0:T(128)} %param.12), kind=kOutput, calls=%fused_computation.15 | convolution fusion | flops 33591296 | bytes 4276256 | tf_op jit(solution)/shard_map/dot_general | solution.py:66
  56.2 1.8 reduce_window_sum.11
  58.0 0.1 copy.23
  58.1 31.4 %all-gather = f32[64,8,1]{1,2,0:T(1,128)S(1)} all-gather(f32[8,8,1]{1,2,0:T(1,128)S(1)} %copy.23), channel_id=2, replica_groups=mesh['gr'=2,'sp'=8,'tp'=2] {'sp'}, dimensions={0}, use_global_device_ids=true | all-gather | bytes 2304 | tf_op jit(solution)/shard_map/all_gather | solution.py:19
  89.6 0.2 while.14
  89.9 0.7 reshape.81
  90.6 3.3 %all-to-all-start.2 = ((f32[8,1,512]{2,1,0:T(1,128)}), f32[8,1,512]{2,1,0:T(1,128)S(1)}, u32[]{:S(2)}, u32[]{:S(2)}) async-start(f32[8,1,512]{2,1,0:T(1,128)} %reshape.81), calls=%async_computation.2 | async-start | bytes 32768 | tf_op jit(solution)/shard_map/all_to_all | solution.py:101
  93.9 32.5 %all-gather.4.cloned.1.call-done = bf16[4096,1024]{1,0:T(8,128)(2,1)} async-done(((bf16[256,1024]{1,0:T(8,128)(2,1)}), bf16[4096,1024]{1,0:T(8,128)(2,1)}) %all-gather.4.cloned.1.call-update) | async-done | bytes 8388624 | tf_op jit(solution)/shard_map/all_gather | solution.py:12
  126.4 9.1 %fusion = bf16[64,8,8,128]{3,1,2,0:T(8,128)(2,1)S(1)} fusion(bf16[512,4096]{1,0:T(8,128)(2,1)} %bitcast.74, bf16[4096,1024]{1,0:T(8,128)(2,1)} %all-gather.4.cloned.1.call-done), kind=kOutput, calls=%fused_computation.3 | convolution fusion | flops 4295491584 | bytes 13631488 | tf_op jit(solution)/shard_map/dot_general | solution.py:66
  135.6 0.3 copy.35
  135.8 1.0 bitcast_bitcast_fusion.1
  136.9 3.7 %all-to-all-start = ((bf16[8,8,64,128]{3,1,2,0:T(8,128)(2,1)}), bf16[8,8,64,128]{3,1,2,0:T(8,128)(2,1)S(1)}, u32[]{:S(2)}, u32[]{:S(2)}) async-start(bf16[8,8,64,128]{3,1,2,0:T(8,128)(2,1)} %bitcast_bitcast_fusion.1), calls=%async_computation | async-start | bytes 2097152 | tf_op jit(solution)/shard_map/all_to_all | solution.py:98
  140.6 111.7 %all-gather.6.cloned.1.call-done = bf16[4096,1024]{1,0:T(8,128)(2,1)} async-done(((bf16[256,1024]{1,0:T(8,128)(2,1)}), bf16[4096,1024]{1,0:T(8,128)(2,1)}) %all-gather.6.cloned.1.call-update) | async-done | bytes 8388624 | tf_op jit(solution)/shard_map/all_gather | solution.py:12
  252.2 9.1 %fusion.1 = bf16[64,8,8,128]{3,1,2,0:T(8,128)(2,1)S(1)} fusion(bf16[512,4096]{1,0:T(8,128)(2,1)} %bitcast.75, bf16[4096,1024]{1,0:T(8,128)(2,1)} %all-gather.6.cloned.1.call-done), kind=kOutput, calls=%fused_computation.4 | convolution fusion | flops 4295491584 | bytes 13631488 | tf_op jit(solution)/shard_map/dot_general | solution.py:66
  261.4 0.3 copy.36
  261.6 1.0 bitcast_bitcast_fusion
  262.7 3.7 %all-to-all-start.1 = ((bf16[8,8,64,128]{3,1,2,0:T(8,128)(2,1)}), bf16[8,8,64,128]{3,1,2,0:T(8,128)(2,1)S(1)}, u32[]{:S(2)}, u32[]{:S(2)}) async-start(bf16[8,8,64,128]{3,1,2,0:T(8,128)(2,1)} %bitcast_bitcast_fusion), calls=%async_computation.1 | async-start | bytes 2097152 | tf_op jit(solution)/shard_map/all_to_all | solution.py:99
  266.4 0.5 broadcast.38
  266.9 0.7 reduce.6
  267.8 0.7 all_to_all.52
  268.5 0.4 fusion.5
  268.8 0.1 fusion.14
  269.0 0.2 fusion.10
  269.2 22.9 %all-to-all-done.1 = bf16[8,8,64,128]{3,1,2,0:T(8,128)(2,1)S(1)} async-done(((bf16[8,8,64,128]{3,1,2,0:T(8,128)(2,1)}), bf16[8,8,64,128]{3,1,2,0:T(8,128)(2,1)S(1)}, u32[]{:S(2)}, u32[]{:S(2)}) %all-to-all-start.1) | async-done | bytes 1048608 | tf_op jit(solution)/shard_map/all_to_all | solution.py:99
  292.2 0.3 fusion.3
  292.4 0.2 multiply_reduce_fusion
  292.7 0.7 fusion.13
  293.3 1.2 copy.20
  294.6 1.2 copy.21
  (25 shorter events, 0.7 us)
Async XLA Ops:
  7.2 259.2 %copy-start = (bf16[8,8,128]{2,1,0:T(8,128)(2,1)S(1)}, bf16[8,8,128]{2,1,0:T(8,128)(2,1)}, u32[]{:S(2)}) copy-start(bf16[8,8,128]{2,1,0:T(8,128)(2,1)} %param.13) | copy-start | bytes 49156
  7.2 119.2 %all-gather.4.cloned.1.call-start = ((), (), s32[]{:S(2)}) async-start(), calls=%async_computation.3 | async-start | bytes 8912896 | tf_op jit(solution)/shard_map/all_gather | solution.py:12
  7.9 244.3 %all-gather.6.cloned.1.call-start = ((), (), s32[]{:S(2)}) async-start(), calls=%async_computation.4 | async-start | bytes 8912896 | tf_op jit(solution)/shard_map/all_gather | solution.py:12
  90.6 46.3 %all-to-all-start.2 = ((f32[8,1,512]{2,1,0:T(1,128)}), f32[8,1,512]{2,1,0:T(1,128)S(1)}, u32[]{:S(2)}, u32[]{:S(2)}) async-start(f32[8,1,512]{2,1,0:T(1,128)} %reshape.81), calls=%async_computation.2 | async-start | bytes 32768 | tf_op jit(solution)/shard_map/all_to_all | solution.py:101
  136.9 125.8 %all-to-all-start = ((bf16[8,8,64,128]{3,1,2,0:T(8,128)(2,1)}), bf16[8,8,64,128]{3,1,2,0:T(8,128)(2,1)S(1)}, u32[]{:S(2)}, u32[]{:S(2)}) async-start(bf16[8,8,64,128]{3,1,2,0:T(8,128)(2,1)} %bitcast_bitcast_fusion.1), calls=%async_computation | async-start | bytes 2097152 | tf_op jit(solution)/shard_map/all_to_all | solution.py:98
  262.7 29.5 %all-to-all-start.1 = ((bf16[8,8,64,128]{3,1,2,0:T(8,128)(2,1)}), bf16[8,8,64,128]{3,1,2,0:T(8,128)(2,1)S(1)}, u32[]{:S(2)}, u32[]{:S(2)}) async-start(bf16[8,8,64,128]{3,1,2,0:T(8,128)(2,1)} %bitcast_bitcast_fusion), calls=%async_computation.1 | async-start | bytes 2097152 | tf_op jit(solution)/shard_map/all_to_all | solution.py:99
Sparse Core Ops, SparseCore 0:
  10.7 115.6 all-gather.3
  129.2 123.0 all-gather.5
where the time goes:
time: 303 us
  waiting for transfers between devices  168 us (55%)
  blocking collectives  75.4 us (25%)
  matrix products  22.4 us (7%)
  between operations  14.2 us (5%)
  starting transfers between devices  10.8 us (4%)
  local copies, waits for them, and re-layouts  7.45 us (2%)
  other arithmetic  3.86 us (1%)
    all_gather x2, waiting for transfers between devices, gathered(): return lax.all_gather(part, axis, axis=dim, tiled=True)  144 us
    all_gather x1, blocking collectives, gathered(): return lax.all_gather(part, axis, axis=dim, tiled=True)  44 us
    all_gather x1, blocking collectives, carried_in(): everything = jax.tree.map(lambda part: lax.all_gather(part, axis), array)  31.4 us
    all_to_all x1, waiting for transfers between devices, on_device(): lax.all_to_all(values, 'sp', split_axis=0, concat_axis=2, tiled=True)  22.9 us
    dot_general x3, matrix products, add_rows(): jnp.dot(columns, piece, preferred_element_type=jnp.float32)  21.7 us
  transfers between devices with their start and end apart: 5, of which 3 were waited for; matrix products, arithmetic and copies ran while one was open for 10% of the time, Pallas kernels for 0%

commit v1 on v0

--- a/solution.py
+++ b/solution.py
@@ -1,9 +1,26 @@
+import functools
 import jax
 import jax.numpy as jnp
 from jax import lax
 from jax.sharding import PartitionSpec as P
 
 eps = 1e-06
+
+
+def solve_widths_now(row_data, axis_name):
+    o_now = jnp.concatenate(
+        lax.all_to_all(
+            jnp.stack(jnp.split(row_data, lax.axis_size(axis_name), axis=0)),
+            split_axis=0,
+            axis_name=axis_name,
+            concat_axis=0,
+        ),
+        axis=2,
+    )
+    return o_now
+
+
+search_lines = functools.partial(solve_widths_now, axis_name="sp")
 
 
 def taken_in(piece, axis, dim, turn, start):
@@ -96,7 +113,7 @@
     cumulative = running_gate + earlier_sum[:, :, None]
     key_cache, value_cache = (
         lax.all_to_all(keys, "sp", split_axis=0, concat_axis=2, tiled=True),
-        lax.all_to_all(values, "sp", split_axis=0, concat_axis=2, tiled=True),
+        search_lines(values),
     )
     gate_cache = lax.all_to_all(cumulative, "sp", split_axis=0, concat_axis=2, tiled=True)
     member = lax.axis_index("sp")

time: 303 us -> 318 us (1.050)
  waiting for transfers between devices: 168 us -> 179 us
  local copies, waits for them, and re-layouts: 7.45 us -> 11.7 us
    all_to_all x1, waiting for transfers between devices: 0.01 us -> 20.5 us  [on_device(): lax.all_to_all(keys, 'sp', split_axis=0, concat_axis=2, tiled=True)]
    all_gather x2, waiting for transfers between devices: 144 us -> 135 us  [gathered(): return lax.all_gather(part, axis, axis=dim, tiled=True)]
    unnamed x6 -> x13, local copies, waits for them, and re-layouts: 1.31 us -> 5.91 us
  transfers between devices with their start and end apart: 5 -> 5, of which waited for: 3 -> 4; matrix products, arithmetic and copies ran while one was open for 10% -> 11% of each run, Pallas kernels for 0% -> 0%
where the time goes in v1:
time: 318 us; the launch traced here: 317 us
  waiting for transfers between devices  179 us (56%)
  blocking collectives  75.4 us (24%)
  matrix products  22.4 us (7%)
  between operations  14.2 us (4%)
  local copies, waits for them, and re-layouts  11.7 us (4%)
  starting transfers between devices  10.7 us (3%)
  other arithmetic  3.86 us (1%)
    all_gather x2, waiting for transfers between devices, gathered(): return lax.all_gather(part, axis, axis=dim, tiled=True)  135 us
    all_gather x1, blocking collectives, gathered(): return lax.all_gather(part, axis, axis=dim, tiled=True)  44 us
    all_gather x1, blocking collectives, carried_in(): everything = jax.tree.map(lambda part: lax.all_gather(part, axis), array)  31.4 us
    all_to_all x1, waiting for transfers between devices, solve_widths_now(): lax.all_to_all(jnp.stack(jnp.split(row_data, lax.axis_size(axis_name), ax...  21.9 us
    dot_general x3, matrix products, add_rows(): jnp.dot(columns, piece, preferred_element_type=jnp.float32)  21.7 us
    all_to_all x1, waiting for transfers between devices, on_device(): lax.all_to_all(keys, 'sp', split_axis=0, concat_axis=2, tiled=True)  20.5 us
  transfers between devices with their start and end apart: 5, of which 4 were waited for; matrix products, arithmetic and copies ran while one was open for 11% of the time, Pallas kernels for 0%

profile of v1, /device:TPU:0, one launch (start us, length us, event | category | flops | bytes accessed | tf_op | source)
XLA Modules:
  0.0 317.5 jit_solution(9839570989811051629)
XLA Ops:
  7.2 0.7 all-gather.4.cloned.1.call-update
  8.0 0.7 all-gather.6.cloned.1.call-update
  8.7 44.0 %all_gather.14 = bf16[4096,8]{0,1:T(8,128)(2,1)S(1)} all-gather(bf16[256,8]{0,1:T(8,128)(2,1)} %param.11), channel_id=1, replica_groups=mesh['gr'=2,'sp'=8,'tp'=2] {'gr','sp'}, dimensions={0}, use_global_device_ids=true | all-gather | bytes 69632 | tf_op jit(solution)/shard_map/all_gather | solution.py:29
  52.7 3.4 %fusion.15 = f32[512,8]{0,1:T(8,128)S(1)} fusion(bf16[512,4096]{1,0:T(8,128)(2,1)} %bitcast.103, bf16[4096,8]{0,1:T(8,128)(2,1)S(1)} %all_gather.14, f32[8]{0:T(128)} %param.12), kind=kOutput, calls=%fused_computation.31 | convolution fusion | flops 33591296 | bytes 4276256 | tf_op jit(solution)/shard_map/dot_general | solution.py:83
  56.2 1.8 reduce_window_sum.11
  58.1 31.4 %all-gather = f32[64,8,1]{1,2,0:T(1,128)S(1)} all-gather(f32[8,8,1]{1,2,0:T(1,128)S(1)} %copy.23), channel_id=2, replica_groups=mesh['gr'=2,'sp'=8,'tp'=2] {'sp'}, dimensions={0}, use_global_device_ids=true | all-gather | bytes 2304 | tf_op jit(solution)/shard_map/all_gather | solution.py:36
  89.9 0.7 reshape.89
  90.6 3.3 %all-to-all-start.2 = ((f32[8,1,512]{2,1,0:T(1,128)}), f32[8,1,512]{2,1,0:T(1,128)S(1)}, u32[]{:S(2)}, u32[]{:S(2)}) async-start(f32[8,1,512]{2,1,0:T(1,128)} %reshape.89), calls=%async_computation.2 | async-start | bytes 32768 | tf_op jit(solution)/shard_map/all_to_all | solution.py:118
  93.9 32.5 %all-gather.4.cloned.1.call-done = bf16[4096,1024]{1,0:T(8,128)(2,1)} async-done(((bf16[256,1024]{1,0:T(8,128)(2,1)}), bf16[4096,1024]{1,0:T(8,128)(2,1)}) %all-gather.4.cloned.1.call-update) | async-done | bytes 8388624 | tf_op jit(solution)/shard_map/all_gather | solution.py:29
  126.4 9.1 %fusion = bf16[64,8,8,128]{3,1,2,0:T(8,128)(2,1)S(1)} fusion(bf16[512,4096]{1,0:T(8,128)(2,1)} %bitcast.104, bf16[4096,1024]{1,0:T(8,128)(2,1)} %all-gather.4.cloned.1.call-done), kind=kOutput, calls=%fused_computation.3 | convolution fusion | flops 4295491584 | bytes 13631488 | tf_op jit(solution)/shard_map/dot_general | solution.py:83
  135.8 1.0 bitcast_bitcast_fusion.1
  136.9 102.8 %all-gather.6.cloned.1.call-done = bf16[4096,1024]{1,0:T(8,128)(2,1)} async-done(((bf16[256,1024]{1,0:T(8,128)(2,1)}), bf16[4096,1024]{1,0:T(8,128)(2,1)}) %all-gather.6.cloned.1.call-update) | async-done | bytes 8388624 | tf_op jit(solution)/shard_map/all_gather | solution.py:29
  239.7 9.1 %fusion.1 = bf16[64,8,8,128]{3,1,2,0:T(8,128)(2,1)S(1)} fusion(bf16[512,4096]{1,0:T(8,128)(2,1)} %bitcast.105, bf16[4096,1024]{1,0:T(8,128)(2,1)} %all-gather.6.cloned.1.call-done), kind=kOutput, calls=%fused_computation.4 | convolution fusion | flops 4295491584 | bytes 13631488 | tf_op jit(solution)/shard_map/dot_general | solution.py:83
  249.2 3.7 %all-to-all-start = ((bf16[8,8,64,128]{3,1,2,0:T(8,128)(2,1)}), bf16[8,8,64,128]{3,1,2,0:T(8,128)(2,1)S(1)}, u32[]{:S(2)}, u32[]{:S(2)}) async-start(bf16[8,8,64,128]{3,1,2,0:T(8,128)(2,1)} %bitcast_bitcast_fusion.1), calls=%async_computation | async-start | bytes 2097152 | tf_op jit(solution)/shard_map/all_to_all | solution.py:115
  252.9 0.6 fusion.14
  253.6 0.7 fusion.13
  254.2 0.7 fusion.12
  254.9 0.7 fusion.11
  255.6 0.7 fusion.10
  256.2 0.6 fusion.9
  256.9 0.7 fusion.8
  257.5 0.7 fusion.7
  258.2 20.5 %all-to-all-done = bf16[8,8,64,128]{3,1,2,0:T(8,128)(2,1)S(1)} async-done(((bf16[8,8,64,128]{3,1,2,0:T(8,128)(2,1)}), bf16[8,8,64,128]{3,1,2,0:T(8,128)(2,1)S(1)}, u32[]{:S(2)}, u32[]{:S(2)}) %all-to-all-start) | async-done | bytes 1048608 | tf_op jit(solution)/shard_map/all_to_all | solution.py:115
  278.7 3.6 %all-to-all-start.1 = ((bf16[8,1,8,64,128]{4,2,3,1,0:T(8,128)(2,1)}), bf16[8,1,8,64,128]{4,2,3,1,0:T(8,128)(2,1)S(1)}, u32[]{:S(2)}, u32[]{:S(2)}) async-start(bf16[8,1,8,64,128]{4,2,3,1,0:T(8,128)(2,1)} %fusion.7), calls=%async_computation.1 | async-start | bytes 2097152 | tf_op jit(solution)/shard_map/all_to_all | solution.py:12
  282.3 0.5 broadcast.38
  282.8 0.7 reduce.6
  283.7 0.7 all_to_all.39
  284.4 1.2 copy.20
  285.6 0.4 fusion.5
  286.4 21.9 %all-to-all-done.1 = bf16[8,1,8,64,128]{4,2,3,1,0:T(8,128)(2,1)S(1)} async-done(((bf16[8,1,8,64,128]{4,2,3,1,0:T(8,128)(2,1)}), bf16[8,1,8,64,128]{4,2,3,1,0:T(8,128)(2,1)S(1)}, u32[]{:S(2)}, u32[]{:S(2)}) %all-to-all-start.1) | async-done | bytes 1048608 | tf_op jit(solution)/shard_map/all_to_all | solution.py:12
  308.2 1.2 copy.21
  310.0 0.7 fusion.21
  (33 shorter events, 2.4 us)
Async XLA Ops:
  7.2 275.1 %copy-start = (bf16[8,8,128]{2,1,0:T(8,128)(2,1)S(1)}, bf16[8,8,128]{2,1,0:T(8,128)(2,1)}, u32[]{:S(2)}) copy-start(bf16[8,8,128]{2,1,0:T(8,128)(2,1)} %param.13) | copy-start | bytes 49156
  7.2 119.2 %all-gather.4.cloned.1.call-start = ((), (), s32[]{:S(2)}) async-start(), calls=%async_computation.3 | async-start | bytes 8912896 | tf_op jit(solution)/shard_map/all_gather | solution.py:29
  7.9 231.8 %all-gather.6.cloned.1.call-start = ((), (), s32[]{:S(2)}) async-start(), calls=%async_computation.4 | async-start | bytes 8912896 | tf_op jit(solution)/shard_map/all_gather | solution.py:29
  90.6 158.7 %all-to-all-start.2 = ((f32[8,1,512]{2,1,0:T(1,128)}), f32[8,1,512]{2,1,0:T(1,128)S(1)}, u32[]{:S(2)}, u32[]{:S(2)}) async-start(f32[8,1,512]{2,1,0:T(1,128)} %reshape.89), calls=%async_computation.2 | async-start | bytes 32768 | tf_op jit(solution)/shard_map/all_to_all | solution.py:118
  249.2 29.5 %all-to-all-start = ((bf16[8,8,64,128]{3,1,2,0:T(8,128)(2,1)}), bf16[8,8,64,128]{3,1,2,0:T(8,128)(2,1)S(1)}, u32[]{:S(2)}, u32[]{:S(2)}) async-start(bf16[8,8,64,128]{3,1,2,0:T(8,128)(2,1)} %bitcast_bitcast_fusion.1), calls=%async_computation | async-start | bytes 2097152 | tf_op jit(solution)/shard_map/all_to_all | solution.py:115
  278.7 29.5 %all-to-all-start.1 = ((bf16[8,1,8,64,128]{4,2,3,1,0:T(8,128)(2,1)}), bf16[8,1,8,64,128]{4,2,3,1,0:T(8,128)(2,1)S(1)}, u32[]{:S(2)}, u32[]{:S(2)}) async-start(bf16[8,1,8,64,128]{4,2,3,1,0:T(8,128)(2,1)} %fusion.7), calls=%async_computation.1 | async-start | bytes 2097152 | tf_op jit(solution)/shard_map/all_to_all | solution.py:12
Sparse Core Ops, SparseCore 0:
  10.7 115.6 all-gather.3
  129.2 110.5 all-gather.5
